TPU v7x, 128 devices: a whole 4x4x4 slice. The times are simulated.
128 devices in a mesh: fs: 16 (over z, y), tp: 8 (over x, core).
Axes of the slice: x: 4, y: 4, z: 4, core: 2. Of those that a mesh axis runs over, the one named last changes fastest.
Arguments:
- tokens: bfloat16 [16384, 2048], P(('fs', 'tp')), may hold values from -6 to 6
- routes: int32 [16384, 4], P(('fs', 'tp')), may hold values from 0 to 127, all different within a row; in each aligned block of 128 rows (0 to 127, 128 to 255, ...) at most 6 rows name the same one
- route_weight: float32 [16384, 4], P(('fs', 'tp')), may hold values from 0.1 to 1
- norm_gain: float32 [2048], P('fs'), may hold values from 0.5 to 4
- gate_weight: float32 [128, 2048, 512], P(None, 'fs', 'tp'), may hold values from -0.125 to 0.125
- up_weight: float32 [128, 2048, 512], P(None, 'fs', 'tp'), may hold values from -0.125 to 0.125
- down_weight: float32 [128, 512, 2048], P(None, 'fs', 'tp'), may hold values from -0.0625 to 0.0625
Outputs:
- gate_new: bfloat16 [128, 2048, 512], P(('fs', 'tp'))
- up_new: bfloat16 [128, 2048, 512], P(('fs', 'tp'))
- down_new: bfloat16 [128, 512, 2048], P(('fs', 'tp'))
- mixed: bfloat16 [16384, 2048], P(('fs', 'tp'))
Inputs may be any that keep to these rules, and one draw needn't show every extreme that they name: `routes`: each row names 4 different experts, and every expert is named by some row; within the 128 rows of one device no expert is named by more than 6 rows, and in some blocks an expert is named by exactly 6 rows.
All inputs are finite; a program needn't handle non-finite values.
Results may differ from a plain program's by a relative error of at most 0.0084.
Values may be sent and summed in bfloat16 or wider, within the bound.
A program may use at most 128 MiB of HBM per device.

v0:
```python
import jax
import jax.numpy as jnp
from jax import lax
from jax.sharding import PartitionSpec as P

norm_epsilon = 1e-06
clamp_limit = 7.0
sigmoid_slope = 1.702


def in_blocks(value, dim, devices):
    before, after = (value.shape[:dim], value.shape[dim + 1 :])
    return jnp.moveaxis(value.reshape(*before, devices, -1, *after), dim, 0)


def joined_along(parts, dim):
    dims = list(parts.shape[1:])
    dims[dim] *= parts.shape[0]
    return jnp.moveaxis(parts, 0, dim).reshape(dims)


def joined_exchange(value, axis, axes, splits, concats):
    sizes = [lax.axis_size(a) for a in axes]
    parts = in_blocks(value, splits[0], sizes[0])
    parts = jnp.moveaxis(in_blocks(parts, splits[1] + 1, sizes[1]), 0, 1)
    inside = parts.shape[2:]
    parts = parts.reshape(-1, *inside)
    parts = lax.all_to_all(parts, axis, split_axis=0, concat_axis=0, tiled=True)
    parts = joined_along(parts.reshape(*sizes, *inside), concats[0] + 1)
    return joined_along(parts, concats[1])


def feed(inputs, gate_mat, up_mat, down_mat):
    gate_pre = jnp.dot(inputs, gate_mat, preferred_element_type=jnp.float32)
    up_pre = jnp.dot(inputs, up_mat, preferred_element_type=jnp.float32)
    gate_part = jnp.minimum(gate_pre, clamp_limit)
    linear_part = jnp.clip(up_pre, -clamp_limit, clamp_limit)
    activation = (
        gate_part * jax.nn.sigmoid(sigmoid_slope * gate_part) * (linear_part + 1.0)
    ).astype(jnp.bfloat16)
    return jnp.dot(activation, down_mat, preferred_element_type=jnp.float32).astype(jnp.bfloat16)


def shards(tokens, routes, route_weight, norm_gain, gate_weight, up_weight, down_weight):
    gain_column = norm_gain[None, :, None]
    gate_tiles = (gate_weight * gain_column).astype(jnp.bfloat16)
    up_tiles = (up_weight * gain_column).astype(jnp.bfloat16)
    down_tiles = down_weight.astype(jnp.bfloat16)
    rows_groups = lax.axis_size("fs")
    column_groups = lax.axis_size("tp")
    gate_new, up_new, down_new = (
        joined_exchange(gate_tiles, ("fs", "tp"), ("fs", "tp"), (0, 0), (1, 2)),
        joined_exchange(up_tiles, ("fs", "tp"), ("fs", "tp"), (0, 0), (1, 2)),
        joined_exchange(down_tiles, ("fs", "tp"), ("fs", "tp"), (0, 0), (1, 2)),
    )
    experts = rows_groups * column_groups
    tok_rows, model_width = tokens.shape
    per_token = routes.shape[1]
    capacity = max(2, 3 * tok_rows * per_token // (2 * experts))
    values = tokens.astype(jnp.float32)
    squares = jnp.mean(values * values, axis=1, keepdims=True)
    normed = (values * lax.rsqrt(squares + norm_epsilon)).astype(jnp.bfloat16)
    flat_routes = routes.reshape(-1)
    onehot = (flat_routes[:, None] == jnp.arange(experts, dtype=jnp.int32)[None, :]).astype(
        jnp.int32
    )
    earlier = jnp.cumsum(onehot, axis=0) - onehot
    rank = jnp.sum(earlier * onehot, axis=1)
    slot_index = flat_routes * capacity + rank
    slot_numbers = jnp.arange(experts * capacity, dtype=jnp.int32)
    select = jnp.any(
        slot_index.reshape(tok_rows, per_token)[None, :, :] == slot_numbers[:, None, None], axis=2
    )
    buffer = jnp.dot(
        select.astype(jnp.bfloat16), normed, preferred_element_type=jnp.float32
    ).astype(jnp.bfloat16)
    buffer = buffer.reshape(experts, 1, capacity, model_width)
    slot_rows = lax.all_to_all(buffer, ("fs", "tp"), split_axis=0, concat_axis=1, tiled=True)
    sources = slot_rows.shape[1]
    count = slot_rows.shape[2]
    expert_out = feed(slot_rows.reshape(-1, model_width), gate_new[0], up_new[0], down_new[0])
    expert_out = expert_out.reshape(1, sources, count, model_width)
    returned = lax.all_to_all(expert_out, ("fs", "tp"), split_axis=1, concat_axis=0, tiled=True)
    returned = returned.reshape(experts * capacity, model_width)
    picked = returned[slot_index].reshape(tok_rows, per_token, model_width)
    mixed = jnp.sum(picked.astype(jnp.float32) * route_weight[:, :, None], axis=1).astype(
        jnp.bfloat16
    )
    return (gate_new, up_new, down_new, mixed)


def solution(mesh):
    placed = (
        P(("fs", "tp"), None),
        P(("fs", "tp"), None),
        P(("fs", "tp"), None),
        P("fs"),
        P(None, "fs", "tp"),
        P(None, "fs", "tp"),
        P(None, "fs", "tp"),
    )
    return jax.shard_map(
        shards,
        mesh=mesh,
        in_specs=placed,
        out_specs=(
            P(("fs", "tp"), None, None),
            P(("fs", "tp"), None, None),
            P(("fs", "tp"), None, None),
            P(("fs", "tp"), None),
        ),
        check_vma=False,
    )
```

profile of v0, /device:TPU:1, one launch (start us, length us, event | category | flops | bytes accessed | tf_op | source)
XLA Modules:
  0.0 281.7 jit_solution(17496281725817418073)
XLA Ops:
  0.6 6.0 %fusion.1 = (bf16[128,1,128,64]{2,3,1,0:T(8,128)(2,1)}, bf16[128,1,128,64]{2,3,1,0:T(8,128)(2,1)S(1)}) fusion(f32[128,128,64]{1,2,0:T(8,128)} %param.12, f32[128]{0:T(128)} %param.10, f32[128,128,64]{1,2,0:T(8,128)} %param.11), kind=kLoop, calls=%fused_computation.7 | loop fusion | flops 4194304 | bytes 12583424 | tf_op jit(solution)/shard_map/reshape;reshape;reshape | solution.py:27
  6.6 41.8 %all_to_all.33 = bf16[128,1,128,64]{2,3,1,0:T(8,128)(2,1)} all-to-all(bf16[128,1,128,64]{2,3,1,0:T(8,128)(2,1)S(1)} %get-tuple-element.27), channel_id=1, replica_groups=mesh['fs'=16,'tp'=8] {'fs','tp'}, dimensions={0} | all-to-all | bytes 4194304 | tf_op jit(solution)/shard_map/all_to_all | solution.py:28
  48.5 4.4 %all-to-all-start.1 = ((bf16[128,1,128,64]{2,3,1,0:T(8,128)(2,1)}), bf16[128,1,128,64]{2,3,1,0:T(8,128)(2,1)S(1)}, u32[]{:S(2)}, u32[]{:S(2)}) async-start(bf16[128,1,128,64]{2,3,1,0:T(8,128)(2,1)} %get-tuple-element.26), calls=%async_computation.1 | async-start | bytes 4194304 | tf_op jit(solution)/shard_map/all_to_all | solution.py:28
  52.9 3.8 %convert_bitcast_fusion = bf16[128,1,32,256]{3,2,1,0:T(8,128)(2,1)} fusion(f32[128,32,256]{2,1,0:T(8,128)} %param.13), kind=kLoop, calls=%fused_computation.10 | loop fusion | flops 1048576 | bytes 6291456 | tf_op jit(solution)/shard_map/reshape;reshape;reshape | solution.py:27
  56.7 26.8 %all-to-all-done.1 = bf16[128,1,128,64]{2,3,1,0:T(8,128)(2,1)S(1)} async-done(((bf16[128,1,128,64]{2,3,1,0:T(8,128)(2,1)}), bf16[128,1,128,64]{2,3,1,0:T(8,128)(2,1)S(1)}, u32[]{:S(2)}, u32[]{:S(2)}) %all-to-all-start.1) | async-done | bytes 2097184 | tf_op jit(solution)/shard_map/all_to_all | solution.py:28
  83.5 5.5 %all-to-all-start.2 = ((bf16[128,1,32,256]{3,2,1,0:T(8,128)(2,1)}), bf16[128,1,32,256]{3,2,1,0:T(8,128)(2,1)}, u32[]{:S(2)}, u32[]{:S(2)}) async-start(bf16[128,1,32,256]{3,2,1,0:T(8,128)(2,1)} %convert_bitcast_fusion), calls=%async_computation.2 | async-start | bytes 4194304 | tf_op jit(solution)/shard_map/all_to_all | solution.py:28
  89.8 0.2 fusion.8
  90.2 0.2 fusion.2
  90.7 2.1 convolution_convert_fusion.1
  92.8 2.9 %reshape.130 = bf16[128,1,6,2048]{3,2,0,1:T(8,128)(2,1)} reshape(bf16[768,2048]{1,0:T(8,128)(2,1)S(1)} %convolution_convert_fusion.1) | data formatting | bytes 6291456 | tf_op jit(solution)/shard_map/reshape | solution.py:77
  95.6 23.6 %all-to-all-done.2 = bf16[128,1,32,256]{3,2,1,0:T(8,128)(2,1)} async-done(((bf16[128,1,32,256]{3,2,1,0:T(8,128)(2,1)}), bf16[128,1,32,256]{3,2,1,0:T(8,128)(2,1)}, u32[]{:S(2)}, u32[]{:S(2)}) %all-to-all-start.2) | async-done | bytes 2097184 | tf_op jit(solution)/shard_map/all_to_all | solution.py:28
  119.2 5.7 %all-to-all-start.3 = ((bf16[128,1,6,2048]{3,2,1,0:T(8,128)(2,1)}), bf16[128,1,6,2048]{3,2,1,0:T(8,128)(2,1)}, u32[]{:S(2)}, u32[]{:S(2)}) async-start(bf16[128,1,6,2048]{3,2,1,0:T(8,128)(2,1)} %bitcast.67), calls=%async_computation.3 | async-start | bytes 8388608 | tf_op jit(solution)/shard_map/all_to_all | solution.py:78
  124.9 2.8 copy.91
  127.7 4.3 %reshape.121 = bf16[8,1,2048,64]{2,3,0,1:T(8,128)(2,1)} reshape(bf16[8,1,16,128,64]{3,2,4,0,1:T(8,128)(2,1)} %bitcast.77) | data formatting | bytes 4194304 | tf_op jit(solution)/shard_map/reshape | solution.py:19
  132.0 2.8 copy.90
  134.7 4.2 %reshape.124 = bf16[8,1,2048,64]{2,3,0,1:T(8,128)(2,1)} reshape(bf16[8,1,16,128,64]{3,2,4,0,1:T(8,128)(2,1)} %bitcast.78) | data formatting | bytes 4194304 | tf_op jit(solution)/shard_map/reshape | solution.py:19
  138.9 1.8 copy.73
  140.8 2.4 copy.74
  143.2 34.5 %all-to-all-done.3 = bf16[128,1,6,2048]{3,2,1,0:T(8,128)(2,1)} async-done(((bf16[128,1,6,2048]{3,2,1,0:T(8,128)(2,1)}), bf16[128,1,6,2048]{3,2,1,0:T(8,128)(2,1)}, u32[]{:S(2)}, u32[]{:S(2)}) %all-to-all-start.3) | async-done | bytes 3145760 | tf_op jit(solution)/shard_map/all_to_all | solution.py:78
  177.6 6.3 %reshape.131 = bf16[768,2048]{1,0:T(8,128)(2,1)} reshape(bf16[128,1,6,2048]{3,2,1,0:T(8,128)(2,1)} %all-to-all-done.3) | data formatting | bytes 6291456 | tf_op jit(solution)/shard_map/reshape | solution.py:81
  184.0 4.8 %fusion.17 = f32[768,512]{1,0:T(8,128)} fusion(bf16[768,2048]{1,0:T(8,128)(2,1)} %reshape.131, bf16[2048,512]{0,1:T(8,128)(2,1)S(1)} %bitcast.71), kind=kOutput, calls=%fused_computation.38 | convolution fusion | flops 1610612736 | bytes 6815744 | tf_op jit(solution)/shard_map/dot_general | solution.py:34
  188.8 9.1 %convolution_convert_fusion = bf16[768,2048]{1,0:T(8,128)(2,1)} fusion(bf16[512,2048]{0,1:T(8,128)(2,1)} %bitcast.75, f32[768,512]{1,0:T(8,128)} %fusion.17, bf16[768,2048]{1,0:T(8,128)(2,1)} %reshape.131, bf16[2048,512]{0,1:T(8,128)(2,1)} %bitcast.73), kind=kOutput, calls=%fused_computation.4 | convolution fusion | flops 3226730496 | bytes 12058624 | tf_op jit(solution)/shard_map/dot_general | solution.py:41
  197.9 6.2 %reshape.132 = bf16[1,128,6,2048]{3,2,1,0:T(8,128)(2,1)} reshape(bf16[768,2048]{1,0:T(8,128)(2,1)} %convolution_convert_fusion) | data formatting | bytes 6291456 | tf_op jit(solution)/shard_map/reshape | solution.py:82
  204.1 5.7 %all-to-all-start.4 = ((bf16[1,128,6,2048]{3,2,0,1:T(8,128)(2,1)}), bf16[1,128,6,2048]{3,2,0,1:T(8,128)(2,1)}, u32[]{:S(2)}, u32[]{:S(2)}) async-start(bf16[1,128,6,2048]{3,2,0,1:T(8,128)(2,1)} %bitcast.68), calls=%async_computation.4 | async-start | bytes 8388608 | tf_op jit(solution)/shard_map/all_to_all | solution.py:83
  210.1 2.5 copy.85
  212.6 4.1 %copy.86 = bf16[1,2048,512]{2,1,0:T(8,128)(2,1)} copy(bf16[1,2048,512]{1,2,0:T(8,128)(2,1)} %bitcast.74) | data formatting | bytes 4194304
  216.6 2.4 copy.87
  219.0 43.5 %all-to-all-done.4 = bf16[1,128,6,2048]{3,2,0,1:T(8,128)(2,1)} async-done(((bf16[1,128,6,2048]{3,2,0,1:T(8,128)(2,1)}), bf16[1,128,6,2048]{3,2,0,1:T(8,128)(2,1)}, u32[]{:S(2)}, u32[]{:S(2)}) %all-to-all-start.4) | async-done | bytes 3145760 | tf_op jit(solution)/shard_map/all_to_all | solution.py:83
  262.5 4.9 %reshape.133 = bf16[768,2048]{1,0:T(8,128)(2,1)S(1)} reshape(bf16[1,128,6,2048]{3,2,0,1:T(8,128)(2,1)} %all-to-all-done.4) | data formatting | bytes 6291456 | tf_op jit(solution)/shard_map/reshape | solution.py:84
  267.4 3.3 %gather_fusion = bf16[512,2048]{1,0:T(8,128)(2,1)} fusion(bf16[768,2048]{1,0:T(8,128)(2,1)S(1)} %reshape.133, s32[1024]{0:T(1024)S(1)} %pad_clamp_fusion), kind=kCustom, calls=%fused_computation | custom fusion | bytes 4196352 | tf_op jit(solution)/shard_map/gather | solution.py:85
  270.7 4.7 %reshape.134 = f32[128,4,2048]{2,1,0:T(4,128)} reshape(bf16[512,2048]{1,0:T(8,128)(2,1)} %gather_fusion) | data formatting | bytes 6291456 | tf_op jit(solution)/shard_map/convert_element_type | solution.py:86
  275.5 6.2 %multiply_reduce_fusion = bf16[128,2048]{1,0:T(8,128)(2,1)} fusion(f32[128,4,2048]{2,1,0:T(4,128)} %reshape.134, f32[128,4]{1,0:T(8,128)S(1)} %copy.84), kind=kLoop, calls=%fused_computation.1 | loop fusion | flops 1835008 | bytes 4720640 | tf_op jit(solution)/shard_map/reduce_sum | solution.py:86
  (36 shorter events, 1.4 us)
Async XLA Ops:
  48.5 35.0 %all-to-all-start.1 = ((bf16[128,1,128,64]{2,3,1,0:T(8,128)(2,1)}), bf16[128,1,128,64]{2,3,1,0:T(8,128)(2,1)S(1)}, u32[]{:S(2)}, u32[]{:S(2)}) async-start(bf16[128,1,128,64]{2,3,1,0:T(8,128)(2,1)} %get-tuple-element.26), calls=%async_computation.1 | async-start | bytes 4194304 | tf_op jit(solution)/shard_map/all_to_all | solution.py:28
  56.7 32.3 %copy-start.6 = (s32[128,4]{0,1:T(4,128)S(1)}, s32[128,4]{0,1:T(4,128)}, u32[]{:S(2)}) copy-start(s32[128,4]{0,1:T(4,128)} %param.8) | copy-start | bytes 6148
  83.5 5.7 %copy-start = (bf16[128,1,128,64]{2,3,1,0:T(8,128)(2,1)}, bf16[128,1,128,64]{2,3,1,0:T(8,128)(2,1)S(1)}, u32[]{:S(2)}) copy-start(bf16[128,1,128,64]{2,3,1,0:T(8,128)(2,1)S(1)} %all-to-all-done.1) | copy-start | bytes 6291460
  83.5 35.8 %all-to-all-start.2 = ((bf16[128,1,32,256]{3,2,1,0:T(8,128)(2,1)}), bf16[128,1,32,256]{3,2,1,0:T(8,128)(2,1)}, u32[]{:S(2)}, u32[]{:S(2)}) async-start(bf16[128,1,32,256]{3,2,1,0:T(8,128)(2,1)} %convert_bitcast_fusion), calls=%async_computation.2 | async-start | bytes 4194304 | tf_op jit(solution)/shard_map/all_to_all | solution.py:28
  89.0 1.5 copy-start.5
  119.2 5.7 %copy-start.2 = (bf16[128,1,128,64]{2,3,1,0:T(8,128)(2,1)S(1)}, bf16[128,1,128,64]{2,3,1,0:T(8,128)(2,1)}, u32[]{:S(2)}) copy-start(bf16[128,1,128,64]{2,3,1,0:T(8,128)(2,1)} %all_to_all.33) | copy-start | bytes 6291460
  119.2 58.4 %all-to-all-start.3 = ((bf16[128,1,6,2048]{3,2,1,0:T(8,128)(2,1)}), bf16[128,1,6,2048]{3,2,1,0:T(8,128)(2,1)}, u32[]{:S(2)}, u32[]{:S(2)}) async-start(bf16[128,1,6,2048]{3,2,1,0:T(8,128)(2,1)} %bitcast.67), calls=%async_computation.3 | async-start | bytes 8388608 | tf_op jit(solution)/shard_map/all_to_all | solution.py:78
  127.7 4.3 %copy-start.1 = (bf16[128,1,128,64]{2,3,1,0:T(8,128)(2,1)S(1)}, bf16[128,1,128,64]{2,3,1,0:T(8,128)(2,1)}, u32[]{:S(2)}) copy-start(bf16[128,1,128,64]{2,3,1,0:T(8,128)(2,1)} %copy-done) | copy-start | bytes 6291460
  143.2 40.8 %copy-start.3 = (bf16[8,1,2048,64]{2,3,0,1:T(8,128)(2,1)S(1)}, bf16[8,1,2048,64]{2,3,0,1:T(8,128)(2,1)}, u32[]{:S(2)}) copy-start(bf16[8,1,2048,64]{2,3,0,1:T(8,128)(2,1)} %reshape.121) | copy-start | bytes 6291460
  204.1 5.8 %copy-start.7 = (f32[128,4]{0,1:T(4,128)S(1)}, f32[128,4]{0,1:T(4,128)}, u32[]{:S(2)}) copy-start(f32[128,4]{0,1:T(4,128)} %param.9) | copy-start | bytes 6148
  204.1 58.4 %all-to-all-start.4 = ((bf16[1,128,6,2048]{3,2,0,1:T(8,128)(2,1)}), bf16[1,128,6,2048]{3,2,0,1:T(8,128)(2,1)}, u32[]{:S(2)}, u32[]{:S(2)}) async-start(bf16[1,128,6,2048]{3,2,0,1:T(8,128)(2,1)} %bitcast.68), calls=%async_computation.4 | async-start | bytes 8388608 | tf_op jit(solution)/shard_map/all_to_all | solution.py:83
  212.6 4.1 %copy-start.4 = (bf16[1,512,8,256]{1,3,2,0:T(8,128)(2,1)S(1)}, bf16[1,512,8,256]{1,3,2,0:T(8,128)(2,1)}, u32[]{:S(2)}) copy-start(bf16[1,512,8,256]{1,3,2,0:T(8,128)(2,1)} %copy.74) | copy-start | bytes 6291460
where the time goes:
time: 283 us; the launch traced here: 282 us
  waiting for transfers between devices  128 us (45%)
  local copies, waits for them, and re-layouts  56.4 us (20%)
  blocking collectives  41.8 us (15%)
  starting transfers between devices  21.3 us (8%)
  other arithmetic  17 us (6%)
  matrix products  16 us (6%)
    all_to_all x2, waiting for transfers between devices, joined_exchange(): parts = lax.all_to_all(parts, axis, split_axis=0, concat_axis=0, tiled=True)  50.4 us
    all_to_all x1, waiting for transfers between devices, shards(): lax.all_to_all(expert_out, ('fs', 'tp'), split_axis=1, concat_axis=0, til...  43.5 us
    all_to_all x1, blocking collectives, joined_exchange(): parts = lax.all_to_all(parts, axis, split_axis=0, concat_axis=0, tiled=True)  41.8 us
    all_to_all x1, waiting for transfers between devices, shards(): lax.all_to_all(buffer, ('fs', 'tp'), split_axis=0, concat_axis=1, tiled=T...  34.5 us
    all_to_all x2, starting transfers between devices, joined_exchange(): parts = lax.all_to_all(parts, axis, split_axis=0, concat_axis=0, tiled=True)  9.91 us
    another operation x2, other arithmetic, joined_exchange(): parts = parts.reshape(-1, *inside)  9.82 us
    unnamed x22, local copies, waits for them, and re-layouts  9.2 us
    dot_general x1, matrix products, feed(): jnp.dot(activation, down_mat, preferred_element_type=jnp.float32)  9.05 us
  transfers between devices with their start and end apart: 4, of which 4 were waited for; matrix products, arithmetic and copies ran while one was open for 13% of the time, Pallas kernels for 0%

commit v1 on v0

v1 whole, which is shorter than its diff:
```python
import jax
import jax.numpy as jnp
from jax import lax
from jax.experimental import pallas as pl
from jax.experimental.pallas import tpu as pltpu
from jax.sharding import PartitionSpec as P

MESH = pl.DeviceIdType.MESH
f32, bf16 = jnp.float32, jnp.bfloat16

norm_epsilon = 1e-06
clamp_limit = 7.0
sigmoid_slope = 1.702

N = 128
D = 2048
FF = 512
CAP = 6
PAD = 8
STRIDE = 101
LOADS = 8
ROWS = 256
GROUP = 16


def offset(k):
    kk = lax.rem(k * STRIDE, N)
    return kk // 32, lax.rem(kk // 8, 4), lax.rem(kk // 2, 4), lax.rem(kk, 2)


def kernel(
    tok, rt, rw, gain, g_in, u_in, d_in,
    g_out, u_out, d_out, m_out,
    g_stage, u_stage, d_stage, wsend, dsend, xsend, xrecv, gu, dn, osend, ret,
    act, gnew, selb, mixw, normed, total,
    load_sem, send_sem, recv_sem, ret_sem, out_sem,
):
    fs, tp = lax.axis_index("fs"), lax.axis_index("tp")
    z, y, x, c = fs // 4, lax.rem(fs, 4), tp // 2, lax.rem(tp, 2)
    me = fs * 8 + tp

    def ahead(k):
        dz, dy, dx, dc = offset(k)
        return (
            lax.rem(z + dz, 4) * 4 + lax.rem(y + dy, 4),
            lax.rem(x + dx, 4) * 2 + lax.rem(c + dc, 2),
        )

    def behind(k):
        dz, dy, dx, dc = offset(k)
        return (
            lax.rem(z + 4 - dz, 4) * 4 + lax.rem(y + 4 - dy, 4),
            lax.rem(x + 4 - dx, 4) * 2 + lax.rem(c + 2 - dc, 2),
        )

    per = N // LOADS

    def load(i, j):
        src, dst = ((g_in, g_stage), (u_in, u_stage), (d_in, d_stage))[j]
        part = pl.ds(i * per, per)
        return pltpu.make_async_copy(src.at[part], dst.at[part], load_sem.at[j, i])

    for i in range(LOADS):
        for j in range(3):
            load(i, j).start()

    barrier = pltpu.get_barrier_semaphore()

    def greet(k, carry):
        pl.semaphore_signal(barrier, inc=1, device_id=ahead(k), device_id_type=MESH)
        return carry

    lax.fori_loop(1, N, greet, 0)

    def iota(shape, dim):
        return lax.broadcasted_iota(jnp.int32, shape, dim)

    kk = (iota((N, N), 0) * STRIDE) & 127
    expert = (
        (((kk >> 5) + z) & 3) * 32
        + (((kk >> 3) + y) & 3) * 8
        + (((kk >> 1) + x) & 3) * 2
        + ((kk + c) & 1)
    )
    named = jnp.zeros((N, N), f32)
    weight = jnp.zeros((N, N), f32)
    for k in range(rt.shape[0]):
        hit = rt[k : k + 1, :] == expert
        named = jnp.where(hit, 1.0, named)
        weight = jnp.where(hit, rw[k : k + 1, :], weight)
    before = jnp.where(iota((N, N), 0) < iota((N, N), 1), 1.0, 0.0).astype(bf16)
    rank = jnp.dot(named.astype(bf16), before, preferred_element_type=f32)
    rank = jnp.where(named > 0.0, rank, -1.0)
    spread = jnp.where(iota((PAD * N, N), 0) // PAD == iota((PAD * N, N), 1), 1.0, 0.0)
    rows = jnp.dot(spread.astype(bf16), rank.astype(bf16), preferred_element_type=f32)
    place = (iota((PAD * N, N), 0) % PAD).astype(f32)
    selb[...] = jnp.where(rows == place, 1.0, 0.0).astype(bf16)

    spread_t = jnp.where(iota((N, PAD * N), 1) // PAD == iota((N, PAD * N), 0), 1.0, 0.0)
    spread_t = spread_t.astype(bf16)
    weight_t = weight.T
    high = weight_t.astype(bf16)
    low = (weight_t - high.astype(f32)).astype(bf16)
    lanes = jnp.dot(rank.T.astype(bf16), spread_t, preferred_element_type=f32)
    hit = lanes == (iota((N, PAD * N), 1) % PAD).astype(f32)
    for i, part in enumerate((high, low)):
        wide = jnp.dot(part, spread_t, preferred_element_type=f32)
        mixw[i * N : (i + 1) * N, :] = jnp.where(hit, wide, 0.0).astype(bf16)

    values = tok[...].astype(f32)
    squares = jnp.mean(values * values, axis=1, keepdims=True)
    normed[...] = (values * lax.rsqrt(squares + norm_epsilon)).astype(bf16)

    def pick(i, carry):
        part = selb[pl.ds(pl.multiple_of(i * N, N), N), :]
        picked = jnp.dot(part, normed[...], preferred_element_type=f32).astype(bf16)
        xsend[pl.ds(i * GROUP, GROUP)] = picked.reshape(GROUP, PAD, D)
        return carry

    lax.fori_loop(0, N // GROUP, pick, 0)

    scale = gain[...].reshape(1, 1, N)
    for i in range(LOADS):
        for j in range(3):
            load(i, j).wait()

        def round_one(e, carry):
            at = pl.ds(i * per + e * 2, 2)
            wsend[at, 0] = (g_stage[at] * scale).astype(bf16)
            wsend[at, 1] = (u_stage[at] * scale).astype(bf16)
            dsend[at] = d_stage[at].astype(bf16)
            return carry

        lax.fori_loop(0, per // 2, round_one, 0)

    pl.semaphore_wait(barrier, N - 1)

    my_rows = pl.ds(pl.multiple_of(tp * 64, 64), 64)
    my_cols = pl.ds(pl.multiple_of(fs * 128, 128), 128)
    down_rows = pl.ds(pl.multiple_of(fs * 32, 32), 32)
    down_cols = pl.ds(pl.multiple_of(tp * 256, 256), 256)

    def remote(src, dst, i, to):
        return pltpu.make_async_remote_copy(
            src_ref=src, dst_ref=dst, send_sem=send_sem.at[i], recv_sem=recv_sem.at[i],
            device_id=to, device_id_type=MESH,
        )

    def send_first(k, carry):
        to = ahead(k)
        t = to[0] * 8 + to[1]
        remote(xsend.at[k, pl.ds(0, CAP)], xrecv.at[k, pl.ds(0, CAP)], 0, to).start()
        remote(wsend.at[t], gu.at[:, my_rows, my_cols], 1, to).start()
        return carry

    def send_second(k, carry):
        to = ahead(k)
        t = to[0] * 8 + to[1]
        remote(dsend.at[t], dn.at[down_rows, down_cols], 2, to).start()
        return carry

    lax.fori_loop(1, N, send_first, 0)
    lax.fori_loop(1, N, send_second, 0)

    xrecv[0] = xsend[0]
    gu[:, my_rows, my_cols] = wsend[me]
    dn[down_rows, down_cols] = dsend[me]

    other = (fs, tp + 1 - 2 * c)
    others = pl.ds(0, N - 1)
    all_rows = remote(xsend.at[others, pl.ds(0, CAP)], xrecv.at[others, pl.ds(0, CAP)], 0, other)
    all_tiles = remote(wsend.at[others], wsend.at[others], 1, other)
    all_down = remote(dsend.at[others], dsend.at[others], 2, other)

    all_rows.wait_recv()
    all_tiles.wait_recv()

    wide = (((1,), (1,)), ((), ()))

    def first(j, carry):
        block = xrecv[pl.ds(j * (ROWS // PAD), ROWS // PAD)].reshape(ROWS, D)
        gate_pre = lax.dot_general(block, gu[0], wide, preferred_element_type=f32)
        up_pre = lax.dot_general(block, gu[1], wide, preferred_element_type=f32)
        gate_part = jnp.minimum(gate_pre, clamp_limit)
        linear_part = jnp.clip(up_pre, -clamp_limit, clamp_limit)
        result = gate_part * jax.nn.sigmoid(sigmoid_slope * gate_part) * (linear_part + 1.0)
        act[pl.ds(pl.multiple_of(j * ROWS, ROWS), ROWS), :] = result.astype(bf16)
        return carry

    lax.fori_loop(0, PAD * N // ROWS, first, 0)

    all_down.wait_recv()

    def back(k, carry):
        pltpu.make_async_remote_copy(
            src_ref=osend.at[k, pl.ds(0, CAP)], dst_ref=ret.at[k, pl.ds(0, CAP)],
            send_sem=send_sem.at[3], recv_sem=ret_sem.at[k // GROUP],
            device_id=behind(k), device_id_type=MESH,
        ).start()
        return carry

    def second(j, carry):
        part = act[pl.ds(pl.multiple_of(j * N, N), N), :]
        result = jnp.dot(part, dn[...], preferred_element_type=f32).astype(bf16)
        osend[pl.ds(j * GROUP, GROUP)] = result.reshape(GROUP, PAD, D)

        @pl.when(j > 0)
        def _():
            lax.fori_loop(lax.max((j - 1) * GROUP, 1), j * GROUP, back, 0)

        return carry

    steps = N // GROUP
    lax.fori_loop(0, steps, second, 0)
    ret[0] = osend[0]
    lax.fori_loop(N - GROUP, N, back, 0)

    for j in range(2):
        def turn(b, carry):
            at = pl.ds(pl.multiple_of(b * 128, 128), 128)
            gnew[j, at, :] = gu[j, :, at].astype(f32).T.astype(bf16)
            return carry

        lax.fori_loop(0, D // 128, turn, 0)

    total[...] = jnp.zeros_like(total)
    outs = (
        pltpu.make_async_copy(gnew.at[0], g_out, out_sem.at[0]),
        pltpu.make_async_copy(gnew.at[1], u_out, out_sem.at[1]),
        pltpu.make_async_copy(dn, d_out, out_sem.at[2]),
    )
    for copy in outs:
        copy.start()

    for j in range(steps):
        count = GROUP - 1 if j == 0 else GROUP
        part = pl.ds(j * GROUP, count)
        pltpu.make_async_remote_copy(
            src_ref=osend.at[part, pl.ds(0, CAP)], dst_ref=ret.at[part, pl.ds(0, CAP)],
            send_sem=send_sem.at[3], recv_sem=ret_sem.at[j],
            device_id=other, device_id_type=MESH,
        ).wait_recv()
        block = ret[j * GROUP : (j + 1) * GROUP]
        block = jnp.where(iota(block.shape, 1) < CAP, block, jnp.zeros_like(block))
        both = jnp.dot(
            mixw[:, j * N : (j + 1) * N], block.reshape(N, D), preferred_element_type=f32
        )
        total[...] += both[:N] + both[N:]
    m_out[...] = total[...].astype(bf16)

    for copy in outs:
        copy.wait()
    all_rows.wait_send()
    all_tiles.wait_send()
    all_down.wait_send()
    remote(osend.at[others, pl.ds(0, CAP)], ret.at[others, pl.ds(0, CAP)], 3, other).wait_send()


def shards(tokens, routes, route_weight, norm_gain, gate_weight, up_weight, down_weight):
    vmem = pl.BlockSpec(memory_space=pltpu.VMEM)
    anywhere = pl.BlockSpec(memory_space=pl.ANY)
    gate_new, up_new, down_new, mixed = pl.pallas_call(
        kernel,
        out_shape=(
            jax.ShapeDtypeStruct((D, FF), bf16),
            jax.ShapeDtypeStruct((D, FF), bf16),
            jax.ShapeDtypeStruct((FF, D), bf16),
            jax.ShapeDtypeStruct((N, D), bf16),
        ),
        in_specs=[vmem, vmem, vmem, vmem, anywhere, anywhere, anywhere],
        out_specs=(anywhere, anywhere, anywhere, vmem),
        scratch_shapes=[
            pltpu.VMEM((N, 64, 128), f32),
            pltpu.VMEM((N, 64, 128), f32),
            pltpu.VMEM((N, 32, 256), f32),
            pltpu.VMEM((N, 2, 64, 128), bf16),
            pltpu.VMEM((N, 32, 256), bf16),
            pltpu.VMEM((N, PAD, D), bf16),
            pltpu.VMEM((N, PAD, D), bf16),
            pltpu.VMEM((2, FF, D), bf16),
            pltpu.VMEM((FF, D), bf16),
            pltpu.VMEM((N, PAD, D), bf16),
            pltpu.VMEM((N, PAD, D), bf16),
            pltpu.VMEM((PAD * N, FF), bf16),
            pltpu.VMEM((2, D, FF), bf16),
            pltpu.VMEM((PAD * N, N), bf16),
            pltpu.VMEM((2 * N, PAD * N), bf16),
            pltpu.VMEM((N, D), bf16),
            pltpu.VMEM((N, D), f32),
            pltpu.SemaphoreType.DMA((3, LOADS)),
            pltpu.SemaphoreType.DMA((4,)),
            pltpu.SemaphoreType.DMA((3,)),
            pltpu.SemaphoreType.DMA((N // GROUP,)),
            pltpu.SemaphoreType.DMA((3,)),
        ],
        compiler_params=pltpu.CompilerParams(
            collective_id=0, has_side_effects=True, vmem_limit_bytes=67043328
        ),
    )(
        tokens,
        routes.T,
        route_weight.T,
        norm_gain.reshape(1, N),
        jnp.swapaxes(gate_weight, 1, 2),
        jnp.swapaxes(up_weight, 1, 2),
        down_weight,
    )
    return gate_new[None], up_new[None], down_new[None], mixed


def solution(mesh):
    placed = (
        P(("fs", "tp"), None),
        P(("fs", "tp"), None),
        P(("fs", "tp"), None),
        P("fs"),
        P(None, "fs", "tp"),
        P(None, "fs", "tp"),
        P(None, "fs", "tp"),
    )
    return jax.shard_map(
        shards,
        mesh=mesh,
        in_specs=placed,
        out_specs=(
            P(("fs", "tp"), None, None),
            P(("fs", "tp"), None, None),
            P(("fs", "tp"), None, None),
            P(("fs", "tp"), None),
        ),
        check_vma=False,
    )
```

time: 283 us -> 184 us (0.65)
  Pallas kernels: 0 us -> 174 us
  waiting for transfers between devices: 128 us -> 0 us
  local copies, waits for them, and re-layouts: 56.4 us -> 7.73 us
  blocking collectives: 41.8 us -> 0 us
  starting transfers between devices: 21.3 us -> 0 us
  other arithmetic: 17 us -> 0 us
  matrix products: 16 us -> 0 us
    pallas_call x0 -> x1, Pallas kernels: none -> 174 us  [shards(): pl.pallas_call(kernel, out_shape=(jax.ShapeDtypeStruct((D, FF), bf16), ja...]
    all_to_all x4 -> x0, waiting for transfers between devices: 128 us -> none  [the longest x2 50.4 us: joined_exchange(): parts = lax.all_to_all(parts, axis, split_axis=0, concat_axis=0, tiled=True)]
    all_to_all x1 -> x0, blocking collectives: 41.8 us -> none  [joined_exchange(): parts = lax.all_to_all(parts, axis, split_axis=0, concat_axis=0, tiled=True)]
    reshape x8 -> x0, local copies, waits for them, and re-layouts: 34.3 us -> none  [the longest x2 8.51 us: joined_along(): return jnp.moveaxis(parts, 0, dim).reshape(dims)]
    all_to_all x4 -> x0, starting transfers between devices: 21.3 us -> none  [the longest x2 9.91 us: joined_exchange(): parts = lax.all_to_all(parts, axis, split_axis=0, concat_axis=0, tiled=True)]
    dot_general x3 -> x0, matrix products: 16 us -> none  [the longest x1 9.05 us: feed(): jnp.dot(activation, down_mat, preferred_element_type=jnp.float32)]
    another operation x5 -> x0, other arithmetic: 10.1 us -> none  [the longest x2 9.82 us: joined_exchange(): parts = parts.reshape(-1, *inside)]
    reduce_sum x3 -> x0, other arithmetic: 6.62 us -> none  [the longest x1 6.2 us: shards(): jnp.sum(picked.astype(jnp.float32) * route_weight[:, :, None], axis=1)]
  transfers between devices with their start and end apart: 4 -> 0, of which waited for: 4 -> 0; matrix products, arithmetic and copies ran while one was open for 13% -> 0% of each run, Pallas kernels for 0% -> 0%
where the time goes in v1:
time: 184 us; the launch traced here: 182 us
  Pallas kernels  174 us (95%)
  local copies, waits for them, and re-layouts  7.73 us (4%)
    pallas_call x1, Pallas kernels, shards(): pl.pallas_call(kernel, out_shape=(jax.ShapeDtypeStruct((D, FF), bf16), ja...  174 us
    unnamed x10, local copies, waits for them, and re-layouts  7.73 us

profile of v1, /device:TPU:1, one launch (start us, length us, event | category | flops | bytes accessed | tf_op | source)
XLA Modules:
  0.0 182.1 jit_solution(2406828581077653869)
XLA Ops:
  0.6 173.7 %shard_map.102 = (bf16[2048,512]{1,0:T(8,128)(2,1)}, bf16[2048,512]{1,0:T(8,128)(2,1)}, bf16[512,2048]{1,0:T(8,128)(2,1)}, bf16[128,2048]{1,0:T(8,128)(2,1)}) custom-call(bf16[128,2048]{1,0:T(8,128)(2,1)} %tok.1, s32[4,128]{1,0:T(4,128)} %bitcast.13, f32[4,128]{1,0:T(4,128)} %bitcast.14, f32[1,128]{1,0:T(1,128)} %bitcast.15, f32[128,64,128]{2,1,0:T(8,128)} %bitcast.8, ...), custom_call_target="tpu_custom_call" | custom-call | tf_op jit(solution)/shard_map/pallas_call | solution.py:262
  174.4 0.0 copy-start.1
  174.4 3.2 %copy.15 = bf16[1,2048,512]{2,1,0:T(8,128)(2,1)} copy(bf16[1,2048,512]{2,1,0:T(8,128)(2,1)} %bitcast.12) | data formatting | bytes 4194304
  177.6 0.0 copy-done.1
  177.6 0.0 copy-start
  177.6 1.3 copy.16
  178.9 1.0 copy-done
  179.9 0.0 copy-start.2
  179.9 1.3 copy.17
  181.2 0.1 copy-done.2
  181.3 0.8 copy.18
Async XLA Ops:
  174.4 3.2 %copy-start.1 = (bf16[2048,512]{1,0:T(8,128)(2,1)S(1)}, bf16[2048,512]{1,0:T(8,128)(2,1)}, u32[]{:S(2)}) copy-start(bf16[2048,512]{1,0:T(8,128)(2,1)} %get-tuple-element.9) | copy-start | bytes 6291460
  177.6 2.3 %copy-start = (bf16[512,2048]{1,0:T(8,128)(2,1)S(1)}, bf16[512,2048]{1,0:T(8,128)(2,1)}, u32[]{:S(2)}) copy-start(bf16[512,2048]{1,0:T(8,128)(2,1)} %get-tuple-element.10) | copy-start | bytes 6291460
  179.9 1.4 copy-start.2

commit v2 on v1

v2 whole, which is shorter than its diff:
```python
import jax
import jax.numpy as jnp
from jax import lax
from jax.experimental import pallas as pl
from jax.experimental.pallas import tpu as pltpu
from jax.sharding import PartitionSpec as P

MESH = pl.DeviceIdType.MESH
f32, bf16 = jnp.float32, jnp.bfloat16

norm_epsilon = 1e-06
clamp_limit = 7.0
sigmoid_slope = 1.702

N = 128
D = 2048
FF = 512
CAP = 6
PAD = 8
STRIDE = 59
LOADS = 8
ROWS = 256
HALF = 64
GROUP = 16


def offset(k):
    kk = lax.rem(k * STRIDE, N)
    return kk // 32, lax.rem(kk // 8, 4), lax.rem(kk // 2, 4), lax.rem(kk, 2)


def kernel(
    tok, rt, rw, gain, g_in, u_in, d_in,
    gate_new, up_new, dn, m_out,
    g_stage, u_stage, d_stage, wsend, dsend, xsend, xrecv, gu, osend, ret,
    act, selb, mixw, normed, total,
    load_sem, send_sem, recv_sem, ret_sem,
):
    fs, tp = lax.axis_index("fs"), lax.axis_index("tp")
    z, y, x, c = fs // 4, lax.rem(fs, 4), tp // 2, lax.rem(tp, 2)
    me = fs * 8 + tp

    def ahead(k):
        dz, dy, dx, dc = offset(k)
        return (
            lax.rem(z + dz, 4) * 4 + lax.rem(y + dy, 4),
            lax.rem(x + dx, 4) * 2 + lax.rem(c + dc, 2),
        )

    def behind(k):
        dz, dy, dx, dc = offset(k)
        return (
            lax.rem(z + 4 - dz, 4) * 4 + lax.rem(y + 4 - dy, 4),
            lax.rem(x + 4 - dx, 4) * 2 + lax.rem(c + 2 - dc, 2),
        )

    per = N // LOADS

    def load(i, j):
        src, dst = ((g_in, g_stage), (u_in, u_stage), (d_in, d_stage))[j]
        part = pl.ds(i * per, per)
        return pltpu.make_async_copy(src.at[part], dst.at[part], load_sem.at[j, i])

    for i in range(LOADS):
        for j in range(3):
            load(i, j).start()

    barrier = pltpu.get_barrier_semaphore()

    def greet(k, carry):
        pl.semaphore_signal(barrier, inc=1, device_id=ahead(k), device_id_type=MESH)
        return carry

    lax.fori_loop(1, N, greet, 0)

    def iota(shape, dim):
        return lax.broadcasted_iota(jnp.int32, shape, dim)

    kk = (iota((N, N), 0) * STRIDE) & 127
    expert = (
        (((kk >> 5) + z) & 3) * 32
        + (((kk >> 3) + y) & 3) * 8
        + (((kk >> 1) + x) & 3) * 2
        + ((kk + c) & 1)
    )
    named = jnp.zeros((N, N), f32)
    weight = jnp.zeros((N, N), f32)
    for k in range(rt.shape[0]):
        hit = rt[k : k + 1, :] == expert
        named = jnp.where(hit, 1.0, named)
        weight = jnp.where(hit, rw[k : k + 1, :], weight)
    before = jnp.where(iota((N, N), 0) < iota((N, N), 1), 1.0, 0.0).astype(bf16)
    rank = jnp.dot(named.astype(bf16), before, preferred_element_type=f32)
    rank = jnp.where(named > 0.0, rank, -1.0)
    spread = jnp.where(iota((PAD * N, N), 0) // PAD == iota((PAD * N, N), 1), 1.0, 0.0)
    rows = jnp.dot(spread.astype(bf16), rank.astype(bf16), preferred_element_type=f32)
    place = (iota((PAD * N, N), 0) % PAD).astype(f32)
    selb[...] = jnp.where(rows == place, 1.0, 0.0).astype(bf16)

    values = tok[...].astype(f32)
    squares = jnp.mean(values * values, axis=1, keepdims=True)
    normed[...] = (values * lax.rsqrt(squares + norm_epsilon)).astype(bf16)

    def pick(i, carry):
        part = selb[pl.ds(pl.multiple_of(i * N, N), N), :]
        picked = jnp.dot(part, normed[...], preferred_element_type=f32).astype(bf16)
        xsend[pl.ds(i * GROUP, GROUP)] = picked.reshape(GROUP, PAD, D)
        return carry

    lax.fori_loop(0, N // GROUP, pick, 0)

    pl.semaphore_wait(barrier, N - 1)

    my_rows = pl.ds(pl.multiple_of(tp * 64, 64), 64)
    my_cols = pl.ds(pl.multiple_of(fs * 128, 128), 128)
    down_rows = pl.ds(pl.multiple_of(fs * 32, 32), 32)
    down_cols = pl.ds(pl.multiple_of(tp * 256, 256), 256)

    def remote(src, dst, i, to):
        return pltpu.make_async_remote_copy(
            src_ref=src, dst_ref=dst, send_sem=send_sem.at[i], recv_sem=recv_sem.at[i],
            device_id=to, device_id_type=MESH,
        )

    def send_rows(half):
        def send(k, carry):
            part = pl.ds(0, CAP)
            remote(xsend.at[k, part], xrecv.at[k, part], half, ahead(k)).start()
            return carry

        return send

    def send_tiles(k, carry):
        to = ahead(k)
        remote(wsend.at[to[0] * 8 + to[1]], gu.at[:, my_rows, my_cols], 2, to).start()
        return carry

    def send_down(k, carry):
        to = ahead(k)
        remote(dsend.at[to[0] * 8 + to[1]], dn.at[down_rows, down_cols], 3, to).start()
        return carry

    lax.fori_loop(1, HALF, send_rows(0), 0)

    scale = gain[...].reshape(1, 1, N)
    for i in range(LOADS):
        for j in range(3):
            load(i, j).wait()

        def round_one(e, carry):
            at = pl.ds(i * per + e * 2, 2)
            wsend[at, 0] = (g_stage[at] * scale).astype(bf16)
            wsend[at, 1] = (u_stage[at] * scale).astype(bf16)
            dsend[at] = d_stage[at].astype(bf16)
            return carry

        lax.fori_loop(0, per // 2, round_one, 0)

    lax.fori_loop(1, N, send_tiles, 0)
    lax.fori_loop(1, N, send_down, 0)
    lax.fori_loop(HALF, N, send_rows(1), 0)

    xrecv[0] = xsend[0]
    gu[:, my_rows, my_cols] = wsend[me]
    dn[down_rows, down_cols] = dsend[me]

    spread_t = jnp.where(iota((N, PAD * N), 1) // PAD == iota((N, PAD * N), 0), 1.0, 0.0)
    spread_t = spread_t.astype(bf16)
    weight_t = weight.T
    high = weight_t.astype(bf16)
    low = (weight_t - high.astype(f32)).astype(bf16)
    lanes = jnp.dot(rank.T.astype(bf16), spread_t, preferred_element_type=f32)
    hit = lanes == (iota((N, PAD * N), 1) % PAD).astype(f32)
    for i, part in enumerate((high, low)):
        wide = jnp.dot(part, spread_t, preferred_element_type=f32)
        mixw[i * N : (i + 1) * N, :] = jnp.where(hit, wide, 0.0).astype(bf16)

    other = (fs, tp + 1 - 2 * c)
    others = pl.ds(0, N - 1)
    early, late = pl.ds(0, HALF - 1), pl.ds(0, N - HALF)
    early_rows = remote(xsend.at[early, pl.ds(0, CAP)], xrecv.at[early, pl.ds(0, CAP)], 0, other)
    late_rows = remote(xsend.at[late, pl.ds(0, CAP)], xrecv.at[late, pl.ds(0, CAP)], 1, other)
    all_tiles = remote(wsend.at[others], wsend.at[others], 2, other)
    all_down = remote(dsend.at[others], dsend.at[others], 3, other)

    wide = (((1,), (1,)), ((), ()))

    def first(j, carry):
        block = xrecv[pl.ds(j * (ROWS // PAD), ROWS // PAD)].reshape(ROWS, D)
        gate_pre = lax.dot_general(block, gu[0], wide, preferred_element_type=f32)
        up_pre = lax.dot_general(block, gu[1], wide, preferred_element_type=f32)
        gate_part = jnp.minimum(gate_pre, clamp_limit)
        linear_part = jnp.clip(up_pre, -clamp_limit, clamp_limit)
        result = gate_part * jax.nn.sigmoid(sigmoid_slope * gate_part) * (linear_part + 1.0)
        act[pl.ds(pl.multiple_of(j * ROWS, ROWS), ROWS), :] = result.astype(bf16)
        return carry

    def back(k, carry):
        pltpu.make_async_remote_copy(
            src_ref=osend.at[k, pl.ds(0, CAP)], dst_ref=ret.at[k, pl.ds(0, CAP)],
            send_sem=send_sem.at[4], recv_sem=ret_sem.at[k // GROUP],
            device_id=behind(k), device_id_type=MESH,
        ).start()
        return carry

    def second(begin):
        def body(j, carry):
            part = act[pl.ds(pl.multiple_of(j * N, N), N), :]
            result = jnp.dot(part, dn[...], preferred_element_type=f32).astype(bf16)
            osend[pl.ds(j * GROUP, GROUP)] = result.reshape(GROUP, PAD, D)

            @pl.when(j > begin)
            def _():
                lax.fori_loop(lax.max((j - 1) * GROUP, 1), j * GROUP, back, 0)

            return carry

        return body

    early_rows.wait_recv()
    all_tiles.wait_recv()
    lax.fori_loop(0, PAD * HALF // ROWS, first, 0)
    all_down.wait_recv()
    lax.fori_loop(0, HALF // GROUP, second(0), 0)
    ret[0] = osend[0]
    lax.fori_loop(HALF - GROUP, HALF, back, 0)

    late_rows.wait_recv()
    lax.fori_loop(PAD * HALF // ROWS, PAD * N // ROWS, first, 0)
    lax.fori_loop(HALF // GROUP, N // GROUP, second(HALF // GROUP), 0)
    lax.fori_loop(N - GROUP, N, back, 0)

    for j, new in enumerate((gate_new, up_new)):
        def turn(b, carry):
            at = pl.ds(pl.multiple_of(b * 128, 128), 128)
            new[at, :] = gu[j, :, at].astype(f32).T.astype(bf16)
            return carry

        lax.fori_loop(0, D // 128, turn, 0)

    total[...] = jnp.zeros_like(total)
    for j in range(N // GROUP):
        count = GROUP - 1 if j == 0 else GROUP
        part = pl.ds(j * GROUP, count)
        pltpu.make_async_remote_copy(
            src_ref=osend.at[part, pl.ds(0, CAP)], dst_ref=ret.at[part, pl.ds(0, CAP)],
            send_sem=send_sem.at[4], recv_sem=ret_sem.at[j],
            device_id=other, device_id_type=MESH,
        ).wait_recv()
        block = ret[j * GROUP : (j + 1) * GROUP]
        block = jnp.where(iota(block.shape, 1) < CAP, block, jnp.zeros_like(block))
        both = jnp.dot(
            mixw[:, j * N : (j + 1) * N], block.reshape(N, D), preferred_element_type=f32
        )
        total[...] += both[:N] + both[N:]
    m_out[...] = total[...].astype(bf16)

    early_rows.wait_send()
    late_rows.wait_send()
    all_tiles.wait_send()
    all_down.wait_send()
    pltpu.make_async_remote_copy(
        src_ref=osend.at[others, pl.ds(0, CAP)], dst_ref=ret.at[others, pl.ds(0, CAP)],
        send_sem=send_sem.at[4], recv_sem=ret_sem.at[0], device_id=other, device_id_type=MESH,
    ).wait_send()


def shards(tokens, routes, route_weight, norm_gain, gate_weight, up_weight, down_weight):
    vmem = pl.BlockSpec(memory_space=pltpu.VMEM)
    anywhere = pl.BlockSpec(memory_space=pl.ANY)
    gate_new, up_new, down_new, mixed = pl.pallas_call(
        kernel,
        out_shape=(
            pltpu.VMEM((D, FF), bf16),
            pltpu.VMEM((D, FF), bf16),
            pltpu.VMEM((FF, D), bf16),
            pltpu.VMEM((N, D), bf16),
        ),
        in_specs=[vmem, vmem, vmem, vmem, anywhere, anywhere, anywhere],
        out_specs=(vmem, vmem, vmem, vmem),
        scratch_shapes=[
            pltpu.VMEM((N, 64, 128), f32),
            pltpu.VMEM((N, 64, 128), f32),
            pltpu.VMEM((N, 32, 256), f32),
            pltpu.VMEM((N, 2, 64, 128), bf16),
            pltpu.VMEM((N, 32, 256), bf16),
            pltpu.VMEM((N, PAD, D), bf16),
            pltpu.VMEM((N, PAD, D), bf16),
            pltpu.VMEM((2, FF, D), bf16),
            pltpu.VMEM((N, PAD, D), bf16),
            pltpu.VMEM((N, PAD, D), bf16),
            pltpu.VMEM((PAD * N, FF), bf16),
            pltpu.VMEM((PAD * N, N), bf16),
            pltpu.VMEM((2 * N, PAD * N), bf16),
            pltpu.VMEM((N, D), bf16),
            pltpu.VMEM((N, D), f32),
            pltpu.SemaphoreType.DMA((3, LOADS)),
            pltpu.SemaphoreType.DMA((5,)),
            pltpu.SemaphoreType.DMA((4,)),
            pltpu.SemaphoreType.DMA((N // GROUP,)),
        ],
        compiler_params=pltpu.CompilerParams(
            collective_id=0, has_side_effects=True, vmem_limit_bytes=55 * 2**20
        ),
    )(
        tokens,
        routes.T,
        route_weight.T,
        norm_gain.reshape(1, N),
        jnp.swapaxes(gate_weight, 1, 2),
        jnp.swapaxes(up_weight, 1, 2),
        down_weight,
    )
    return gate_new[None], up_new[None], down_new[None], mixed


def solution(mesh):
    placed = (
        P(("fs", "tp"), None),
        P(("fs", "tp"), None),
        P(("fs", "tp"), None),
        P("fs"),
        P(None, "fs", "tp"),
        P(None, "fs", "tp"),
        P(None, "fs", "tp"),
    )
    return jax.shard_map(
        shards,
        mesh=mesh,
        in_specs=placed,
        out_specs=(
            P(("fs", "tp"), None, None),
            P(("fs", "tp"), None, None),
            P(("fs", "tp"), None, None),
            P(("fs", "tp"), None),
        ),
        check_vma=False,
    )
```

time: 184 us -> 162 us (0.88)
  Pallas kernels: 174 us -> 155 us
  local copies, waits for them, and re-layouts: 7.73 us -> 4.75 us
    pallas_call x1, Pallas kernels: 174 us -> 155 us  [shards(): pl.pallas_call(kernel, out_shape=(pltpu.VMEM((D, FF), bf16), pltpu.VMEM((...]
    unnamed x10 -> x4, local copies, waits for them, and re-layouts: 7.73 us -> 4.75 us
where the time goes in v2:
time: 162 us; the launch traced here: 161 us
  Pallas kernels  155 us (96%)
  local copies, waits for them, and re-layouts  4.75 us (3%)
    pallas_call x1, Pallas kernels, shards(): pl.pallas_call(kernel, out_shape=(pltpu.VMEM((D, FF), bf16), pltpu.VMEM((...  155 us
    unnamed x4, local copies, waits for them, and re-layouts  4.75 us

profile of v2, /device:TPU:1, one launch (start us, length us, event | category | flops | bytes accessed | tf_op | source)
XLA Modules:
  0.0 160.5 jit_solution(4779213642353167850)
XLA Ops:
  0.6 155.1 %shard_map.102 = (bf16[2048,512]{1,0:T(8,128)(2,1)S(1)}, bf16[2048,512]{1,0:T(8,128)(2,1)S(1)}, bf16[512,2048]{1,0:T(8,128)(2,1)S(1)}, bf16[128,2048]{1,0:T(8,128)(2,1)S(1)}) custom-call(bf16[128,2048]{1,0:T(8,128)(2,1)} %tok.1, s32[4,128]{1,0:T(4,128)} %bitcast.13, f32[4,128]{1,0:T(4,128)} %bitcast.14, f32[1,128]{1,0:T(1,128)} %bitcast.15, ...), custom_call_target="tpu_custom_call" | custom-call | tf_op jit(solution)/shard_map/pallas_call | solution.py:271
  155.8 1.3 copy.15
  157.1 1.3 copy.16
  158.4 0.8 copy.18
  159.2 1.3 copy.17

commit v3 on v2

--- a/solution.py
+++ b/solution.py
@@ -265,10 +265,19 @@
     ).wait_send()
 
 
+def write(*refs):
+    sem = refs[8]
+    copies = [pltpu.make_async_copy(refs[i], refs[4 + i], sem.at[i]) for i in range(4)]
+    for copy in copies:
+        copy.start()
+    for copy in copies:
+        copy.wait()
+
+
 def shards(tokens, routes, route_weight, norm_gain, gate_weight, up_weight, down_weight):
     vmem = pl.BlockSpec(memory_space=pltpu.VMEM)
     anywhere = pl.BlockSpec(memory_space=pl.ANY)
-    gate_new, up_new, down_new, mixed = pl.pallas_call(
+    held = pl.pallas_call(
         kernel,
         out_shape=(
             pltpu.VMEM((D, FF), bf16),
@@ -311,6 +320,15 @@
         jnp.swapaxes(up_weight, 1, 2),
         down_weight,
     )
+    held = [pltpu.with_memory_space_constraint(array, pltpu.VMEM) for array in held]
+    gate_new, up_new, down_new, mixed = pl.pallas_call(
+        write,
+        out_shape=[jax.ShapeDtypeStruct(array.shape, bf16) for array in held],
+        in_specs=[vmem] * 4,
+        out_specs=[anywhere] * 4,
+        scratch_shapes=[pltpu.SemaphoreType.DMA((4,))],
+        compiler_params=pltpu.CompilerParams(vmem_limit_bytes=2**20),
+    )(*held)
     return gate_new[None], up_new[None], down_new[None], mixed
 
 

time: 162 us -> 160 us (0.988)
  local copies, waits for them, and re-layouts: 4.75 us -> 0 us
  Pallas kernels: 155 us -> 158 us
    unnamed x4 -> x0, local copies, waits for them, and re-layouts: 4.75 us -> none
    pallas_call x0 -> x1, Pallas kernels: none -> 2.84 us  [shards(): pl.pallas_call(write, out_shape=[jax.ShapeDtypeStruct(array.shape, bf16)...]
where the time goes in v3:
time: 160 us; the launch traced here: 159 us
  Pallas kernels  158 us (99%)
    pallas_call x1, Pallas kernels, shards(): pl.pallas_call(kernel, out_shape=(pltpu.VMEM((D, FF), bf16), pltpu.VMEM((...  155 us

profile of v3, /device:TPU:1, one launch (start us, length us, event | category | flops | bytes accessed | tf_op | source)
XLA Modules:
  0.0 158.6 jit_solution(1626197873431478342)
XLA Ops:
  0.6 155.1 %shard_map.102 = (bf16[2048,512]{1,0:T(8,128)(2,1)S(1)}, bf16[2048,512]{1,0:T(8,128)(2,1)S(1)}, bf16[512,2048]{1,0:T(8,128)(2,1)S(1)}, bf16[128,2048]{1,0:T(8,128)(2,1)S(1)}) custom-call(bf16[128,2048]{1,0:T(8,128)(2,1)} %tok.1, s32[4,128]{1,0:T(4,128)} %bitcast.10, f32[4,128]{1,0:T(4,128)} %bitcast.11, f32[1,128]{1,0:T(1,128)} %bitcast.12, ...), custom_call_target="tpu_custom_call" | custom-call | tf_op jit(solution)/shard_map/pallas_call | solution.py:280
  155.8 2.8 %shard_map.103 = (bf16[2048,512]{1,0:T(8,128)(2,1)}, bf16[2048,512]{1,0:T(8,128)(2,1)}, bf16[512,2048]{1,0:T(8,128)(2,1)}, bf16[128,2048]{1,0:T(8,128)(2,1)}) custom-call(bf16[2048,512]{1,0:T(8,128)(2,1)S(1)} %get-tuple-element.12.refs_0_, bf16[2048,512]{1,0:T(8,128)(2,1)S(1)} %get-tuple-element.13.refs_1_, bf16[512,2048]{1,0:T(8,128)(2,1)S(1)} %get-tuple-element.14.refs_2_, ...), custom_call_target="tpu_custom_call" | custom-call | tf_op jit(solution)/shard_map/pallas_call | solution.py:324

commit v4 on v3

--- a/solution.py
+++ b/solution.py
@@ -17,7 +17,7 @@
 FF = 512
 CAP = 6
 PAD = 8
-STRIDE = 59
+STRIDE = 47
 LOADS = 8
 ROWS = 256
 HALF = 64
@@ -54,6 +54,14 @@
             lax.rem(x + 4 - dx, 4) * 2 + lax.rem(c + 2 - dc, 2),
         )
 
+    barrier = pltpu.get_barrier_semaphore()
+
+    def greet(k, carry):
+        pl.semaphore_signal(barrier, inc=1, device_id=ahead(k), device_id_type=MESH)
+        return carry
+
+    lax.fori_loop(1, N, greet, 0)
+
     per = N // LOADS
 
     def load(i, j):
@@ -64,14 +72,6 @@
     for i in range(LOADS):
         for j in range(3):
             load(i, j).start()
-
-    barrier = pltpu.get_barrier_semaphore()
-
-    def greet(k, carry):
-        pl.semaphore_signal(barrier, inc=1, device_id=ahead(k), device_id_type=MESH)
-        return carry
-
-    lax.fori_loop(1, N, greet, 0)
 
     def iota(shape, dim):
         return lax.broadcasted_iota(jnp.int32, shape, dim)
@@ -109,39 +109,6 @@
 
     lax.fori_loop(0, N // GROUP, pick, 0)
 
-    pl.semaphore_wait(barrier, N - 1)
-
-    my_rows = pl.ds(pl.multiple_of(tp * 64, 64), 64)
-    my_cols = pl.ds(pl.multiple_of(fs * 128, 128), 128)
-    down_rows = pl.ds(pl.multiple_of(fs * 32, 32), 32)
-    down_cols = pl.ds(pl.multiple_of(tp * 256, 256), 256)
-
-    def remote(src, dst, i, to):
-        return pltpu.make_async_remote_copy(
-            src_ref=src, dst_ref=dst, send_sem=send_sem.at[i], recv_sem=recv_sem.at[i],
-            device_id=to, device_id_type=MESH,
-        )
-
-    def send_rows(half):
-        def send(k, carry):
-            part = pl.ds(0, CAP)
-            remote(xsend.at[k, part], xrecv.at[k, part], half, ahead(k)).start()
-            return carry
-
-        return send
-
-    def send_tiles(k, carry):
-        to = ahead(k)
-        remote(wsend.at[to[0] * 8 + to[1]], gu.at[:, my_rows, my_cols], 2, to).start()
-        return carry
-
-    def send_down(k, carry):
-        to = ahead(k)
-        remote(dsend.at[to[0] * 8 + to[1]], dn.at[down_rows, down_cols], 3, to).start()
-        return carry
-
-    lax.fori_loop(1, HALF, send_rows(0), 0)
-
     scale = gain[...].reshape(1, 1, N)
     for i in range(LOADS):
         for j in range(3):
@@ -155,6 +122,39 @@
             return carry
 
         lax.fori_loop(0, per // 2, round_one, 0)
+
+    pl.semaphore_wait(barrier, N - 1)
+
+    my_rows = pl.ds(pl.multiple_of(tp * 64, 64), 64)
+    my_cols = pl.ds(pl.multiple_of(fs * 128, 128), 128)
+    down_rows = pl.ds(pl.multiple_of(fs * 32, 32), 32)
+    down_cols = pl.ds(pl.multiple_of(tp * 256, 256), 256)
+
+    def remote(src, dst, i, to):
+        return pltpu.make_async_remote_copy(
+            src_ref=src, dst_ref=dst, send_sem=send_sem.at[i], recv_sem=recv_sem.at[i],
+            device_id=to, device_id_type=MESH,
+        )
+
+    def send_rows(half):
+        def send(k, carry):
+            part = pl.ds(0, CAP)
+            remote(xsend.at[k, part], xrecv.at[k, part], half, ahead(k)).start()
+            return carry
+
+        return send
+
+    def send_tiles(k, carry):
+        to = ahead(k)
+        remote(wsend.at[to[0] * 8 + to[1]], gu.at[:, my_rows, my_cols], 2, to).start()
+        return carry
+
+    def send_down(k, carry):
+        to = ahead(k)
+        remote(dsend.at[to[0] * 8 + to[1]], dn.at[down_rows, down_cols], 3, to).start()
+        return carry
+
+    lax.fori_loop(1, HALF, send_rows(0), 0)
 
     lax.fori_loop(1, N, send_tiles, 0)
     lax.fori_loop(1, N, send_down, 0)

time: 160 us -> 158 us (0.988)
  no operation moved by 1% of the time
where the time goes in v4:
time: 158 us
  Pallas kernels  157 us (99%)
    pallas_call x1, Pallas kernels, shards(): pl.pallas_call(kernel, out_shape=(pltpu.VMEM((D, FF), bf16), pltpu.VMEM((...  154 us

profile of v4, /device:TPU:1, one launch (start us, length us, event | category | flops | bytes accessed | tf_op | source)
XLA Modules:
  0.0 157.9 jit_solution(10673526563911549088)
XLA Ops:
  0.6 154.4 %shard_map.102 = (bf16[2048,512]{1,0:T(8,128)(2,1)S(1)}, bf16[2048,512]{1,0:T(8,128)(2,1)S(1)}, bf16[512,2048]{1,0:T(8,128)(2,1)S(1)}, bf16[128,2048]{1,0:T(8,128)(2,1)S(1)}) custom-call(bf16[128,2048]{1,0:T(8,128)(2,1)} %tok.1, s32[4,128]{1,0:T(4,128)} %bitcast.10, f32[4,128]{1,0:T(4,128)} %bitcast.11, f32[1,128]{1,0:T(1,128)} %bitcast.12, ...), custom_call_target="tpu_custom_call" | custom-call | tf_op jit(solution)/shard_map/pallas_call | solution.py:280
  155.0 2.8 %shard_map.103 = (bf16[2048,512]{1,0:T(8,128)(2,1)}, bf16[2048,512]{1,0:T(8,128)(2,1)}, bf16[512,2048]{1,0:T(8,128)(2,1)}, bf16[128,2048]{1,0:T(8,128)(2,1)}) custom-call(bf16[2048,512]{1,0:T(8,128)(2,1)S(1)} %get-tuple-element.12.refs_0_, bf16[2048,512]{1,0:T(8,128)(2,1)S(1)} %get-tuple-element.13.refs_1_, bf16[512,2048]{1,0:T(8,128)(2,1)S(1)} %get-tuple-element.14.refs_2_, ...), custom_call_target="tpu_custom_call" | custom-call | tf_op jit(solution)/shard_map/pallas_call | solution.py:324
